TPU v7x, 512 devices: a whole 4x8x8 slice. The times are simulated.
512 devices in a mesh: ep: 32 (over z, x), tp: 16 (over y, core).
Axes of the slice: x: 4, y: 8, z: 8, core: 2. Of those that a mesh axis runs over, the one named last changes fastest.
Arguments:
- queries: bfloat16 [4096, 512], P('ep'), may hold values from -6 to 6
- key_vectors: bfloat16 [4096, 512], P('ep'), may hold values from -6 to 6
- values: bfloat16 [4096, 1024], P('ep', 'tp'), may hold values from -6 to 6
- out_gate: bfloat16 [4096, 1024], P('ep', 'tp'), may hold values from -6 to 6
- input_gate: float32 [4096, 2], P('ep'), may hold values from -8 to 130
- forget_gate: float32 [4096, 2], P('ep'), may hold values from -2 to 16
- mix_weight: bfloat16 [1024, 2048], P('tp'), may hold values from -0.1875 to 0.1875
- expert_input: bfloat16 [8192, 2048], P('ep'), may hold values from -6 to 6
- norm_gain: float32 [2048], replicated, may hold values from 0.1 to 1.9
- route_ids: int32 [8192, 4], P('ep'), may hold values from 0 to 63, all different within a row; in each aligned block of 256 rows (0 to 255, 256 to 511, ...) at most 32 rows name the same one
- route_weights: float32 [8192, 4], P('ep'), may hold values from 0.2 to 1.2
- expert_gate: bfloat16 [512, 2048, 128], P(('ep', 'tp')), may hold values from -0.125 to 0.125
- expert_up: bfloat16 [512, 2048, 128], P(('ep', 'tp')), may hold values from -0.125 to 0.125
- expert_down: bfloat16 [512, 128, 2048], P(('ep', 'tp')), may hold values from -0.1875 to 0.1875
- shared_gate: bfloat16 [2048, 512], P(None, 'tp'), may hold values from -0.125 to 0.125
- shared_up: bfloat16 [2048, 512], P(None, 'tp'), may hold values from -0.125 to 0.125
- shared_down: bfloat16 [512, 2048], P('tp'), may hold values from -0.25 to 0.25
Outputs:
- mixer_out: bfloat16 [4096, 2048], P('ep')
- expert_out: bfloat16 [8192, 2048], P('ep')
Inputs may be any that keep to these rules, and one draw needn't show every extreme that they name: `route_ids`: each row names 4 different experts. In each aligned block of 256 rows (the rows of one index of ep) no expert is named by more than 32 rows, and in some block one expert is named by exactly 32 rows.
All inputs are finite; a program needn't handle non-finite values.
Results may differ from a plain program's by a relative error of at most 0.01575.
Values may be sent and summed in bfloat16 or wider, within the bound.
A program may use at most 64 MiB of HBM per device.

v0:
```python
import jax
import jax.numpy as jnp
from jax import lax
from jax.sharding import Mesh
from jax.sharding import PartitionSpec as P

D = 2048
MEMORY_HEADS = 2
KEY_DIM = 256
BLOCK = 128
FF = 1024
EP = ("ep_0", "ep_1")
EP_TP = ("ep_0", "ep_1", "tp")
epsilon = 1e-06
lowest = -1e30
den_floor = 4.0


def nothing_yet(array, identity):
    return jax.tree.map(
        lambda part, zero: jnp.zeros_like(part) + jnp.asarray(zero, part.dtype), array, identity
    )


def all_in_one(array, axis):
    leaves = jax.tree.leaves(array)
    order = sorted(range(len(leaves)), key=lambda k: -leaves[k].size)
    width = (1, *leaves[order[0]].shape)[-1]
    lines = [
        jnp.pad(leaves[k].reshape(-1), (0, -leaves[k].size % width)).reshape(-1, width)
        for k in order
    ]
    both, at, found = (lax.all_gather(jnp.concatenate(lines), axis), 0, {})
    for k, line in zip(order, lines):
        section = both[:, at : at + len(line)].reshape(len(both), -1)
        found[k] = section[:, : leaves[k].size].reshape(-1, *leaves[k].shape)
        at += len(line)
    numbers = iter(range(len(leaves)))
    return jax.tree.map(lambda _: found[next(numbers)], array)


def entering_2(array, axes, combine, identity):
    before = start = nothing_yet(array, identity)
    subtotal = array
    for axis in reversed(axes):
        count, place = (lax.axis_size(axis), lax.axis_index(axis))
        pieces = all_in_one(subtotal, axis)
        inside, subtotal = (start, start)
        for k in range(count):
            passed = k < place
            subtotal = combine(subtotal, jax.tree.map(lambda part: part[k], pieces))
            inside = jax.tree.map(lambda new, old: jnp.where(passed, new, old), subtotal, inside)
        before = combine(inside, before)
    return before


def in_blocks(array, dim, count):
    before, after = (array.shape[:dim], array.shape[dim + 1 :])
    return jnp.moveaxis(array.reshape(*before, count, -1, *after), dim, 0)


def summed_on_arrival(array, axis, dim):
    blocks = in_blocks(array, dim, lax.axis_size(axis))
    arrived = lax.all_to_all(blocks, axis, split_axis=0, concat_axis=0, tiled=True)
    return arrived.astype(jnp.float32).sum(axis=0)


def from_everyone(array, axis):
    copies = jnp.broadcast_to(array, (lax.axis_size(axis), *array.shape))
    return lax.all_to_all(copies, axis, split_axis=0, concat_axis=0, tiled=True)


def in_order(blocks, dim):
    blocks = jnp.moveaxis(blocks, 0, dim)
    shape = blocks.shape
    return blocks.reshape(*shape[:dim], shape[dim] * shape[dim + 1], *shape[dim + 2 :])


def collect(array, axis, dim):
    blocks = from_everyone(array, axis)
    return in_order(blocks, dim)


def combine_segments(earlier, later):
    first_decay, first_memory, first_normalizer, first_running = earlier
    second_decay, second_memory, second_normalizer, second_running = later
    running = jnp.maximum(second_decay + first_running, second_running)
    lead_scale = jnp.exp(second_decay + first_running - running)
    tail_scale = jnp.exp(second_running - running)
    return (
        first_decay + second_decay,
        lead_scale * first_memory + tail_scale * second_memory,
        lead_scale * first_normalizer + tail_scale * second_normalizer,
        running,
    )


def mixer_half(queries, key_vectors, values, out_gate, input_gate, forget_gate, mix_weight):
    tp_count = lax.axis_size("tp")
    tp_rank = lax.axis_index("tp")
    length = queries.shape[0]
    blocks = length // BLOCK
    channels = values.shape[1]
    factor = KEY_DIM ** (-0.5)
    head_index = tp_rank // (tp_count // MEMORY_HEADS)
    offset = head_index * KEY_DIM
    query_head = lax.dynamic_slice_in_dim(queries, offset, KEY_DIM, 1).reshape(
        blocks, BLOCK, KEY_DIM
    )
    key_head = lax.dynamic_slice_in_dim(key_vectors, offset, KEY_DIM, 1).reshape(
        blocks, BLOCK, KEY_DIM
    )
    value_blocks = values.reshape(blocks, BLOCK, channels)
    select = jnp.arange(MEMORY_HEADS, dtype=jnp.int32)[None, :] == head_index
    input_head = jnp.sum(jnp.where(select, input_gate, 0.0), axis=1).reshape(blocks, BLOCK)
    forget_head = jax.nn.log_sigmoid(jnp.sum(jnp.where(select, forget_gate, 0.0), axis=1)).reshape(
        blocks, BLOCK
    )
    cumulative = jnp.cumsum(forget_head, axis=1)
    block_total = cumulative[:, -1]
    log_retention = block_total[:, None] - cumulative + input_head
    block_running = jnp.max(log_retention, axis=1)
    weighted_keys = (
        key_head.astype(jnp.float32) * jnp.exp(log_retention - block_running[:, None])[:, :, None]
    )
    block_memory = jnp.einsum(
        "bsd,bsv->bdv",
        weighted_keys,
        value_blocks.astype(jnp.float32),
        precision=lax.Precision.HIGHEST,
    )
    block_normalizer = jnp.sum(weighted_keys, axis=1)
    segments = (block_total, block_memory, block_normalizer, block_running)
    neutral = (
        jnp.zeros((), jnp.float32),
        jnp.zeros((KEY_DIM, channels), jnp.float32),
        jnp.zeros((KEY_DIM,), jnp.float32),
        jnp.full((), lowest, jnp.float32),
    )

    def fold_block(carry_in, segment):
        return (combine_segments(carry_in, segment), None)

    summary, _ = lax.scan(fold_block, neutral, segments)
    prefix = entering_2(summary, EP, combine_segments, neutral)
    start_state = (
        jnp.zeros((), jnp.float32),
        jnp.zeros((KEY_DIM, channels), jnp.float32),
        jnp.zeros((KEY_DIM,), jnp.float32),
        jnp.zeros((), jnp.float32),
    )
    entering = combine_segments(start_state, prefix)
    causal = jnp.tril(jnp.ones((BLOCK, BLOCK), dtype=bool))

    def block_pass(carry_in, inputs):
        query_block, key_block, value_block, input_block, cumulative_block, segment = inputs
        _, memory, normalizer, running = carry_in
        carried = cumulative_block + running
        log_weight = cumulative_block[:, None] - cumulative_block[None, :] + input_block[None, :]
        log_weight = jnp.where(causal, log_weight, -jnp.inf)
        stabilizer = jnp.maximum(carried, jnp.max(log_weight, axis=1))
        within = jnp.exp(log_weight - stabilizer[:, None])
        across = jnp.exp(carried - stabilizer)
        scores = (
            jnp.einsum("td,sd->ts", query_block, key_block, preferred_element_type=jnp.float32)
            * factor
        )
        weights = scores * within
        scaled = query_block.astype(jnp.float32) * factor
        numerator = across[:, None] * jnp.dot(scaled, memory, precision=lax.Precision.HIGHEST)
        numerator = numerator + jnp.dot(
            weights.astype(jnp.bfloat16), value_block, preferred_element_type=jnp.float32
        )
        denominator = across * jnp.dot(scaled, normalizer, precision=lax.Precision.HIGHEST)
        denominator = denominator + jnp.sum(weights, axis=1)
        hidden = numerator / jnp.maximum(jnp.abs(denominator), den_floor)[:, None]
        return (combine_segments(carry_in, segment), hidden)

    _, hidden = lax.scan(
        block_pass, entering, (query_head, key_head, value_blocks, input_head, cumulative, segments)
    )
    gated_rows = (
        hidden.reshape(length, channels) * jax.nn.sigmoid(out_gate.astype(jnp.float32))
    ).astype(jnp.bfloat16)
    return jnp.dot(gated_rows, mix_weight, preferred_element_type=jnp.float32)


def expert_half(
    expert_input,
    norm_gain,
    route_ids,
    route_weights,
    expert_gate,
    expert_up,
    expert_down,
    shared_gate,
    shared_up,
    shared_down,
):
    ep_count = lax.axis_size(EP)
    tp_count = lax.axis_size("tp")
    tp_rank = lax.axis_index("tp")
    tokens = expert_input.shape[0]
    top_count = route_ids.shape[1]
    slice_units = expert_gate.shape[2]
    group_size = FF // slice_units
    per_ep = tp_count // group_size
    team_index = tp_rank // group_size
    expert_count = ep_count * per_ep
    capacity = 2 * tokens * top_count // expert_count
    rows_wide = expert_input.astype(jnp.float32)
    normed = (
        rows_wide
        * lax.rsqrt(jnp.mean(rows_wide * rows_wide, axis=-1, keepdims=True) + epsilon)
        * norm_gain
    ).astype(jnp.bfloat16)
    chosen = route_ids.reshape(-1)
    onehot = (chosen[:, None] == jnp.arange(expert_count, dtype=jnp.int32)[None, :]).astype(
        jnp.int32
    )
    slot_rank = jnp.sum((jnp.cumsum(onehot, axis=0) - onehot) * onehot, axis=1)
    in_team = chosen % per_ep == team_index
    target = jnp.where(in_team, chosen // per_ep * capacity + slot_rank, ep_count * capacity)
    token_of = jnp.arange(chosen.shape[0], dtype=jnp.int32) // top_count
    slot_token = jnp.zeros((ep_count * capacity,), jnp.int32).at[target].set(token_of, mode="drop")
    slot_live = jnp.zeros((ep_count * capacity,), jnp.int32).at[target].set(1, mode="drop")
    outgoing = jnp.where(slot_live[:, None] > 0, normed[slot_token], jnp.zeros((), jnp.bfloat16))
    outgoing = outgoing.reshape(ep_count, capacity, D)
    gate_slice = expert_gate[0]
    up_slice = expert_up[0]
    down_slice = expert_down[0]
    arrived = lax.all_to_all(outgoing, EP, split_axis=0, concat_axis=0, tiled=True)
    gate_val = jnp.einsum("sid,df->sif", arrived, gate_slice, preferred_element_type=jnp.float32)
    up_val = jnp.einsum("sid,df->sif", arrived, up_slice, preferred_element_type=jnp.float32)
    hidden = (jax.nn.silu(gate_val) * up_val).astype(jnp.bfloat16)
    partial_value = jnp.einsum(
        "sif,fd->sid", hidden, down_slice, preferred_element_type=jnp.float32
    )
    partial_value = partial_value.astype(jnp.bfloat16)
    returned = lax.all_to_all(partial_value, EP, split_axis=0, concat_axis=0, tiled=True)
    flat_back = returned.reshape(ep_count * capacity, returned.shape[2])
    gather_at = jnp.where(in_team, target, 0).reshape(tokens, top_count)
    weight_at = jnp.where(in_team, route_weights.reshape(-1), 0.0).reshape(tokens, top_count)
    combined = jnp.zeros((tokens, returned.shape[2]), jnp.float32)
    for pick_index in range(top_count):
        combined = (
            combined
            + flat_back[gather_at[:, pick_index]].astype(jnp.float32)
            * weight_at[:, pick_index][:, None]
        )
    shared_gate_val = jnp.dot(normed, shared_gate, preferred_element_type=jnp.float32)
    shared_up_val = jnp.dot(normed, shared_up, preferred_element_type=jnp.float32)
    shared_act = (jax.nn.silu(shared_gate_val) * shared_up_val).astype(jnp.bfloat16)
    return combined + jnp.dot(shared_act, shared_down, preferred_element_type=jnp.float32)


def shards(
    queries,
    key_vectors,
    values,
    out_gate,
    input_gate,
    forget_gate,
    mix_weight,
    expert_input,
    norm_gain,
    route_ids,
    route_weights,
    expert_gate,
    expert_up,
    expert_down,
    shared_gate,
    shared_up,
    shared_down,
):
    mixer_partial = mixer_half(
        queries, key_vectors, values, out_gate, input_gate, forget_gate, mix_weight
    )
    expert_partial = expert_half(
        expert_input,
        norm_gain,
        route_ids,
        route_weights,
        expert_gate,
        expert_up,
        expert_down,
        shared_gate,
        shared_up,
        shared_down,
    )
    mixer_piece = summed_on_arrival(mixer_partial.astype(jnp.bfloat16), "tp", 0).astype(
        jnp.bfloat16
    )
    mixer_out = lax.all_gather(mixer_piece, "tp", axis=0, tiled=True)
    expert_piece = lax.psum_scatter(expert_partial, "tp", scatter_dimension=0, tiled=True).astype(
        jnp.bfloat16
    )
    expert_out = collect(expert_piece, "tp", 0)
    return (mixer_out, expert_out)


def solution(mesh):
    finer = Mesh(mesh.devices.reshape(8, 4, mesh.shape["tp"]), ("ep_0", "ep_1", "tp"))
    placed = (
        P(EP, None),
        P(EP, None),
        P(EP, "tp"),
        P(EP, "tp"),
        P(EP, None),
        P(EP, None),
        P("tp", None),
        P(EP, None),
        P(),
        P(EP, None),
        P(EP, None),
        P(EP_TP, None, None),
        P(EP_TP, None, None),
        P(EP_TP, None, None),
        P(None, "tp"),
        P(None, "tp"),
        P("tp", None),
    )
    return jax.shard_map(
        shards, mesh=finer, in_specs=placed, out_specs=(P(EP, None), P(EP, None)), check_vma=False
    )
```

profile of v0, /device:TPU:1, one launch (start us, length us, event | category | flops | bytes accessed | tf_op | source)
XLA Modules:
  0.0 426.6 jit_solution(15270256443497055373)
XLA Ops:
  7.2 0.9 copy.108
  8.6 18.0 %reduce-window.6 = s32[64,8,128]{2,1,0:T(8,128)S(1)} reduce-window(s32[64,8,128]{2,1,0:T(8,128)S(1)} %fusion.29, s32[]{:T(128)} %constant.140.clone.1), window={size=1x1x128 pad=0_0x0_0x127_0}, to_apply=%region_8.9 | reduce-window | flops 8323072 | bytes 524292 | tf_op jit(solution)/shard_map/reduce-window
  27.3 4.3 %scatter_custom_fusion.1 = s32[1024]{0:T(1024)S(1)} fusion(s32[1024]{0:T(1024)S(1)} %bitcast.173, s32[1024]{0:T(1024)S(1)} %add_select_fusion.3, s32[]{:T(128)} %constant.140.clone.1), kind=kCustom, calls=%fused_computation.234 | custom fusion | bytes 4100 | tf_op jit(solution)/shard_map/scatter | solution.py:225
  31.6 0.3 fusion.1
  31.9 4.3 %scatter_custom_fusion = s32[1024]{0:T(1024)S(1)} fusion(s32[1024]{0:T(1024)S(1)} %bitcast.174, s32[1024]{0:T(1024)S(1)} %broadcast.491, s32[]{:T(128)} %constant.140.clone.1), kind=kCustom, calls=%fused_computation.237 | custom fusion | bytes 4100 | tf_op jit(solution)/shard_map/scatter | solution.py:226
  36.3 0.3 fusion.3
  36.6 6.0 %gather_fusion = bf16[1024,2048]{1,0:T(8,128)(2,1)} fusion(bf16[256,2048]{1,0:T(8,128)(2,1)S(1)} %fusion.3, s32[1024]{0:T(1024)S(1)} %fusion.157), kind=kCustom, calls=%fused_computation | custom fusion | bytes 8392704 | tf_op jit(solution)/shard_map/gather | solution.py:227
  42.7 2.5 broadcast_select_fusion
  45.2 107.2 %all_to_all.20 = bf16[32,32,2048]{2,1,0:T(8,128)(2,1)S(1)} all-to-all(bf16[32,32,2048]{2,1,0:T(8,128)(2,1)S(1)} %broadcast_select_fusion), channel_id=1, replica_groups=mesh['ep_0'=8,'ep_1'=4,'tp'=16] {'ep_0','ep_1'}, dimensions={0} | all-to-all | bytes 8388608 | tf_op jit(solution)/shard_map/all_to_all | solution.py:232
  152.5 1.9 copy-done.1
  154.4 1.2 fusion.18
  155.7 8.5 %convolution_convert_fusion = bf16[32,32,2048]{2,1,0:T(8,128)(2,1)} fusion(bf16[32,32,2048]{2,1,0:T(8,128)(2,1)} %copy-done.1, bf16[1,128,2048]{2,1,0:T(8,128)(2,1)S(1)} %copy-done, bf16[1,2048,128]{2,1,0:T(8,128)(2,1)S(1)} %copy-done.4, f32[32,32,128]{2,1,0:T(8,128)S(1)} %fusion.18), kind=kOutput, calls=%fused_computation.8 | convolution fusion | flops 1076625408 | bytes 9961472 | tf_op jit(solution)/shard_map/sif,fd->sid/dot_general | solution.py:236
  164.2 6.7 %all-to-all-start.2 = ((bf16[32,32,2048]{2,1,0:T(8,128)(2,1)}), bf16[32,32,2048]{2,1,0:T(8,128)(2,1)}, u32[]{:S(2)}, u32[]{:S(2)}) async-start(bf16[32,32,2048]{2,1,0:T(8,128)(2,1)} %convolution_convert_fusion), calls=%async_computation.2 | async-start | bytes 8388608 | tf_op jit(solution)/shard_map/all_to_all | solution.py:240
  171.2 0.3 reduce_window_sum.26
  171.5 0.6 slice.281
  172.7 1.2 fusion.178
  175.4 1.3 subtract_exponential_fusion.1
  177.1 0.6 pad_bitcast_fusion.3
  178.2 20.0 %all-gather.2 = f32[4,262,64]{1,2,0:T(8,128)S(1)} all-gather(f32[1,262,64]{1,2,0:T(8,128)S(1)} %maximum_bitcast_fusion), channel_id=2, replica_groups=mesh['ep_0'=8,'ep_1'=4,'tp'=16] {'ep_1'}, dimensions={0}, use_global_device_ids=true | all-gather | bytes 335360 | tf_op jit(solution)/shard_map/all_gather | solution.py:33
  198.5 0.6 fusion.185
  208.8 0.3 copy-done.13
  209.4 0.6 copy-done.19
  211.3 0.7 copy.96
  212.1 0.3 fusion.33
  212.5 0.6 pad_clamp_fusion.2
  213.1 0.6 pad_clamp_fusion
  213.8 0.9 slice_reduce_fusion.3
  214.7 0.4 fusion.188
  215.1 48.3 %all-to-all-done.2 = bf16[32,32,2048]{2,1,0:T(8,128)(2,1)} async-done(((bf16[32,32,2048]{2,1,0:T(8,128)(2,1)}), bf16[32,32,2048]{2,1,0:T(8,128)(2,1)}, u32[]{:S(2)}, u32[]{:S(2)}) %all-to-all-start.2) | async-done | bytes 4194336 | tf_op jit(solution)/shard_map/all_to_all | solution.py:240
  263.5 5.2 %gather_fusion.1 = bf16[256,2048]{1,0:T(8,128)(2,1)S(1)} fusion(bf16[1024,2048]{1,0:T(8,128)(2,1)} %bitcast.58, s32[1024]{0:T(1024)} %get-tuple-element.135), kind=kCustom, calls=%fused_computation.1 | custom fusion | bytes 2098176 | tf_op jit(solution)/shard_map/gather | solution.py:248
  268.7 6.2 %gather_fusion.2 = bf16[256,2048]{1,0:T(8,128)(2,1)} fusion(bf16[1024,2048]{1,0:T(8,128)(2,1)} %bitcast.58, s32[1024]{0:T(1024)} %get-tuple-element.134), kind=kCustom, calls=%fused_computation.2 | custom fusion | bytes 2098176 | tf_op jit(solution)/shard_map/gather | solution.py:248
  274.9 6.2 %gather_fusion.3 = bf16[256,2048]{1,0:T(8,128)(2,1)} fusion(bf16[1024,2048]{1,0:T(8,128)(2,1)} %bitcast.58, s32[1024]{0:T(1024)} %get-tuple-element.133), kind=kCustom, calls=%fused_computation.3 | custom fusion | bytes 2098176 | tf_op jit(solution)/shard_map/gather | solution.py:248
  281.2 6.2 %gather_fusion.4 = bf16[256,2048]{1,0:T(8,128)(2,1)} fusion(bf16[1024,2048]{1,0:T(8,128)(2,1)} %bitcast.58, s32[1024]{0:T(1024)} %get-tuple-element.132), kind=kCustom, calls=%fused_computation.4 | custom fusion | bytes 2098176 | tf_op jit(solution)/shard_map/gather | solution.py:248
  287.4 5.0 %convolution_add_fusion = f32[256,2048]{1,0:T(8,128)} fusion(bf16[32,2048]{1,0:T(8,128)(2,1)S(1)} %copy-done.6, bf16[256,2048]{1,0:T(8,128)(2,1)} %gather_fusion.4, bf16[256,2048]{1,0:T(8,128)(2,1)} %gather_fusion.3, bf16[256,2048]{1,0:T(8,128)(2,1)} %gather_fusion.2, bf16[256,2048]{1,0:T(8,128)(2,1)S(1)} %gather_fusion.1, bf16[256,2048]{1,0:T(8,128)(2,1)S(1)} %fusion.3, ...), kind=kOutput, calls=%fused_computation.9 | convolution fusion | flops 73449472 | bytes 7639040 | tf_op jit(solution)/shard_map/dot_general | solution.py:254
  292.6 0.6 copy-done.10
  293.3 21.1 %all-gather.3 = f32[8,262,64]{1,2,0:T(8,128)S(1)} all-gather(f32[1,262,64]{1,2,0:T(8,128)S(1)} %maximum_bitcast_fusion.1), channel_id=3, replica_groups=mesh['ep_0'=8,'ep_1'=4,'tp'=16] {'ep_0'}, dimensions={0}, use_global_device_ids=true | all-gather | bytes 603648 | tf_op jit(solution)/shard_map/all_gather | solution.py:33
  314.7 0.6 fusion.184
  316.1 0.6 fusion.183
  340.4 0.4 convolution_multiply_fusion.4
  340.8 1.3 fusion
  342.1 16.0 %all-to-all-start = ((bf16[16,8,2048]{2,1,0:T(8,128)(2,1)}), bf16[16,8,2048]{2,1,0:T(8,128)(2,1)S(1)}, u32[]{:S(2)}, u32[]{:S(2)}) async-start(bf16[16,8,2048]{2,1,0:T(8,128)(2,1)} %fusion), calls=%async_computation | async-start | bytes 1048576 | tf_op jit(solution)/shard_map/all_to_all | solution.py:64
  358.1 0.9 convert_element_type.83
  359.0 16.3 %all-to-all-done = bf16[16,8,2048]{2,1,0:T(8,128)(2,1)S(1)} async-done(((bf16[16,8,2048]{2,1,0:T(8,128)(2,1)}), bf16[16,8,2048]{2,1,0:T(8,128)(2,1)S(1)}, u32[]{:S(2)}, u32[]{:S(2)}) %all-to-all-start) | async-done | bytes 524320 | tf_op jit(solution)/shard_map/all_to_all | solution.py:64
  375.3 1.1 broadcast_in_dim.93
  376.4 3.6 all-to-all-start.3
  380.0 37.9 %all_gather.19 = bf16[128,2048]{1,0:T(8,128)(2,1)S(1)} all-gather(bf16[8,2048]{1,0:T(8,128)(2,1)S(1)} %reduce_sum.75), channel_id=1, replica_groups=mesh['ep_0'=8,'ep_1'=4,'tp'=16] {'tp'}, dimensions={0}, use_global_device_ids=true | all-gather | bytes 557056 | tf_op jit(solution)/shard_map/all_gather | solution.py:294
  418.0 0.8 copy.149
  418.8 1.0 copy.150
  (135 shorter events, 6.0 us)
Async XLA Ops:
  7.2 148.5 %copy-start = (bf16[1,128,2048]{2,1,0:T(8,128)(2,1)S(1)}, bf16[1,128,2048]{2,1,0:T(8,128)(2,1)}, u32[]{:S(2)}) copy-start(bf16[1,128,2048]{2,1,0:T(8,128)(2,1)} %param.30) | copy-start | bytes 1572868
  7.2 24.4 %copy-start.2 = (bf16[256,2048]{1,0:T(8,128)(2,1)S(1)}, bf16[256,2048]{1,0:T(8,128)(2,1)}, u32[]{:S(2)}) copy-start(bf16[256,2048]{1,0:T(8,128)(2,1)} %param.24) | copy-start | bytes 3145732
  7.2 29.1 %copy-start.25 = (f32[2048]{0:T(1024)S(1)}, f32[2048]{0:T(1024)}, u32[]{:S(2)}) copy-start(f32[2048]{0:T(1024)} %param.25) | copy-start | bytes 24580
  45.2 109.2 %copy-start.3 = (bf16[1,2048,128]{2,1,0:T(8,128)(2,1)S(1)}, bf16[1,2048,128]{2,1,0:T(8,128)(2,1)}, u32[]{:S(2)}) copy-start(bf16[1,2048,128]{2,1,0:T(8,128)(2,1)} %param.28) | copy-start | bytes 1572868
  152.5 1.9 copy-start.1
  154.4 1.3 copy-start.4
  164.2 6.9 %copy-start.29 = (f32[128,2]{0,1:T(2,128)S(1)}, f32[128,2]{0,1:T(2,128)}, u32[]{:S(2)}) copy-start(f32[128,2]{0,1:T(2,128)} %param.21) | copy-start | bytes 3076
  164.2 6.9 %copy-start.30 = (f32[128,2]{0,1:T(2,128)S(1)}, f32[128,2]{0,1:T(2,128)}, u32[]{:S(2)}) copy-start(f32[128,2]{0,1:T(2,128)} %param.22) | copy-start | bytes 3076
  164.2 12.5 %copy-start.9 = (bf16[128,512]{1,0:T(8,128)(2,1)S(1)}, bf16[128,512]{1,0:T(8,128)(2,1)}, u32[]{:S(2)}) copy-start(bf16[128,512]{1,0:T(8,128)(2,1)} %param.18) | copy-start | bytes 393220
  164.2 13.7 %copy-start.11 = (bf16[128,64]{0,1:T(8,128)(2,1)S(1)}, bf16[128,64]{0,1:T(8,128)(2,1)}, u32[]{:S(2)}) copy-start(bf16[128,64]{0,1:T(8,128)(2,1)} %param.19) | copy-start | bytes 49156
  164.2 43.6 %copy-start.22 = (s32[256,4]{0,1:T(4,128)S(1)}, s32[256,4]{0,1:T(4,128)}, u32[]{:S(2)}) copy-start(s32[256,4]{0,1:T(4,128)} %param.26) | copy-start | bytes 12292
  164.2 43.8 %copy-start.28 = (f32[256,4]{0,1:T(4,128)S(1)}, f32[256,4]{0,1:T(4,128)}, u32[]{:S(2)}) copy-start(f32[256,4]{0,1:T(4,128)} %param.27) | copy-start | bytes 12292
  164.2 99.3 %all-to-all-start.2 = ((bf16[32,32,2048]{2,1,0:T(8,128)(2,1)}), bf16[32,32,2048]{2,1,0:T(8,128)(2,1)}, u32[]{:S(2)}, u32[]{:S(2)}) async-start(bf16[32,32,2048]{2,1,0:T(8,128)(2,1)} %convolution_convert_fusion), calls=%async_computation.2 | async-start | bytes 8388608 | tf_op jit(solution)/shard_map/all_to_all | solution.py:240
  170.9 187.2 %reduce-scatter.2.cloned.1.call-start = ((), (), s32[]{:S(2)}) async-start(), calls=%async_computation.5 | async-start | bytes 2228224 | tf_op jit(solution)/shard_map/reduce_scatter | solution.py:295
  171.2 5.6 %copy-start.26 = (f32[128]{0:T(128)}, f32[128]{0:T(128)S(1)}, u32[]{:S(2)}) copy-start(f32[128]{0:T(128)S(1)} %get-tuple-element.69) | copy-start | bytes 1540
  171.5 37.0 %copy-start.23 = (f32[1,128]{1,0:T(1,128)}, f32[1,128]{1,0:T(1,128)S(1)}, u32[]{:S(2)}) copy-start(f32[1,128]{1,0:T(1,128)S(1)} %reduce_window_sum.26) | copy-start | bytes 1540
  177.9 36.9 %copy-start.8 = (bf16[2048,32]{0,1:T(8,128)(2,1)S(1)}, bf16[2048,32]{0,1:T(8,128)(2,1)}, u32[]{:S(2)}) copy-start(bf16[2048,32]{0,1:T(8,128)(2,1)} %param.31) | copy-start | bytes 393220
  208.6 0.6 copy-start.13
  208.7 0.6 copy-start.15
  208.8 0.6 copy-start.17
  209.4 0.6 copy-start.19
  281.2 6.2 %copy-start.6 = (bf16[32,2048]{1,0:T(8,128)(2,1)S(1)}, bf16[32,2048]{1,0:T(8,128)(2,1)}, u32[]{:S(2)}) copy-start(bf16[32,2048]{1,0:T(8,128)(2,1)} %param.33) | copy-start | bytes 393220
  281.2 6.2 %copy-start.7 = (bf16[2048,32]{0,1:T(8,128)(2,1)S(1)}, bf16[2048,32]{0,1:T(8,128)(2,1)}, u32[]{:S(2)}) copy-start(bf16[2048,32]{0,1:T(8,128)(2,1)} %param.32) | copy-start | bytes 393220
  292.4 0.8 copy-start.10
  292.5 47.1 %copy-start.14 = (f32[1,4,64]{2,1,0:T(4,128)S(1)}, f32[1,4,64]{2,1,0:T(4,128)}, u32[]{:S(2)}) copy-start(f32[1,4,64]{2,1,0:T(4,128)} %copy-done.13) | copy-start | bytes 3076
  292.5 47.1 %copy-start.16 = (f32[1,4,64]{2,1,0:T(4,128)S(1)}, f32[1,4,64]{2,1,0:T(4,128)}, u32[]{:S(2)}) copy-start(f32[1,4,64]{2,1,0:T(4,128)} %copy-done.15) | copy-start | bytes 3076
  292.5 47.1 %copy-start.18 = (f32[1,4,64]{2,1,0:T(4,128)S(1)}, f32[1,4,64]{2,1,0:T(4,128)}, u32[]{:S(2)}) copy-start(f32[1,4,64]{2,1,0:T(4,128)} %copy-done.17) | copy-start | bytes 3076
  292.5 47.1 %copy-start.20 = (f32[1,4,64]{2,1,0:T(4,128)S(1)}, f32[1,4,64]{2,1,0:T(4,128)}, u32[]{:S(2)}) copy-start(f32[1,4,64]{2,1,0:T(4,128)} %copy-done.19) | copy-start | bytes 3076
  292.5 47.3 %copy-start.24 = (f32[1,128]{1,0:T(1,128)S(1)}, f32[1,128]{1,0:T(1,128)}, u32[]{:S(2)}) copy-start(f32[1,128]{1,0:T(1,128)} %copy-done.23) | copy-start | bytes 1540
  292.5 47.3 %copy-start.27 = (f32[128]{0:T(128)S(1)}, f32[128]{0:T(128)}, u32[]{:S(2)}) copy-start(f32[128]{0:T(128)} %copy-done.26) | copy-start | bytes 1540
  292.5 47.5 %copy-start.12 = (bf16[128,512]{1,0:T(8,128)(2,1)S(1)}, bf16[128,512]{1,0:T(8,128)(2,1)}, u32[]{:S(2)}) copy-start(bf16[128,512]{1,0:T(8,128)(2,1)} %param.17) | copy-start | bytes 393220
  314.3 26.5 %copy-start.5 = (bf16[64,2048]{1,0:T(8,128)(2,1)S(1)}, bf16[64,2048]{1,0:T(8,128)(2,1)}, u32[]{:S(2)}) copy-start(bf16[64,2048]{1,0:T(8,128)(2,1)} %param.23) | copy-start | bytes 786436
  314.4 26.5 %copy-start.21 = (bf16[128,64]{0,1:T(8,128)(2,1)S(1)}, bf16[128,64]{0,1:T(8,128)(2,1)}, u32[]{:S(2)}) copy-start(bf16[128,64]{0,1:T(8,128)(2,1)} %param.20) | copy-start | bytes 49156
  342.1 33.2 %all-to-all-start = ((bf16[16,8,2048]{2,1,0:T(8,128)(2,1)}), bf16[16,8,2048]{2,1,0:T(8,128)(2,1)S(1)}, u32[]{:S(2)}, u32[]{:S(2)}) async-start(bf16[16,8,2048]{2,1,0:T(8,128)(2,1)} %fusion), calls=%async_computation | async-start | bytes 1048576 | tf_op jit(solution)/shard_map/all_to_all | solution.py:64
  376.4 41.6 %all-to-all-start.3 = ((bf16[16,16,2048]{2,1,0:T(8,128)(2,1)}), bf16[16,16,2048]{2,1,0:T(8,128)(2,1)S(1)}, u32[]{:S(2)}, u32[]{:S(2)}) async-start(bf16[16,16,2048]{2,1,0:T(8,128)(2,1)} %broadcast_in_dim.93), calls=%async_computation.4 | async-start | bytes 2097152 | tf_op jit(solution)/shard_map/all_to_all | solution.py:70
Sparse Core Ops, SparseCore 0:
  292.6 61.3 reduce-scatter.1
where the time goes:
time: 428 us; the launch traced here: 427 us
  blocking collectives  186 us (43%)
  waiting for transfers between devices  64.6 us (15%)
  local copies, waits for them, and re-layouts  54.5 us (13%)
  between operations  49.7 us (12%)
  other arithmetic  27.8 us (6%)
  starting transfers between devices  26.2 us (6%)
  matrix products  17.5 us (4%)
    all_to_all x1, blocking collectives, expert_half(): lax.all_to_all(outgoing, EP, split_axis=0, concat_axis=0, tiled=True)  107 us
    all_to_all x1, waiting for transfers between devices, expert_half(): lax.all_to_all(partial_value, EP, split_axis=0, concat_axis=0, tiled=True)  48.3 us
    all_gather x2, blocking collectives, all_in_one(): both, at, found = (lax.all_gather(jnp.concatenate(lines), axis), 0, {})  41.1 us
    all_gather x1, blocking collectives, shards(): mixer_out = lax.all_gather(mixer_piece, 'tp', axis=0, tiled=True)  37.9 us
    gather x4, local copies, waits for them, and re-layouts, expert_half(): flat_back[gather_at[:, pick_index]].astype(jnp.float32)  23.9 us
    another operation x3, other arithmetic  18.2 us
    all_to_all x1, waiting for transfers between devices, summed_on_arrival(): lax.all_to_all(blocks, axis, split_axis=0, concat_axis=0, tiled=True)  16.3 us
    all_to_all x1, starting transfers between devices, summed_on_arrival(): lax.all_to_all(blocks, axis, split_axis=0, concat_axis=0, tiled=True)  16 us
  transfers between devices with their start and end apart: 4, of which 2 were waited for; matrix products, arithmetic and copies ran while one was open for 4% of the time, Pallas kernels for 0%

commit v1 on v0

--- a/solution.py
+++ b/solution.py
@@ -291,7 +291,9 @@
     mixer_piece = summed_on_arrival(mixer_partial.astype(jnp.bfloat16), "tp", 0).astype(
         jnp.bfloat16
     )
-    mixer_out = lax.all_gather(mixer_piece, "tp", axis=0, tiled=True)
+    mixer_out = jnp.concatenate(
+        lax.all_to_all(jnp.stack([mixer_piece] * lax.axis_size("tp")), "tp", 0, 0), axis=0
+    )
     expert_piece = lax.psum_scatter(expert_partial, "tp", scatter_dimension=0, tiled=True).astype(
         jnp.bfloat16
     )

time: 428 us -> 462 us (1.079)
  blocking collectives: 186 us -> 228 us
  starting transfers between devices: 26.2 us -> 18.9 us
    all_to_all x1, waiting for transfers between devices: 48.3 us -> 0.01 us  [expert_half(): lax.all_to_all(partial_value, EP, split_axis=0, concat_axis=0, tiled=True)]
    all_gather x2, blocking collectives: 41.1 us -> 88 us  [all_in_one(): both, at, found = (lax.all_gather(jnp.concatenate(lines), axis), 0, {})]
    all_gather x1 -> x0, blocking collectives: 37.9 us -> none  [shards(): mixer_out = lax.all_gather(mixer_piece, 'tp', axis=0, tiled=True)]
    reduce_scatter x1, waiting for transfers between devices: 0.01 us -> 34.1 us  [shards(): lax.psum_scatter(expert_partial, 'tp', scatter_dimension=0, tiled=True)]
    all_to_all x0 -> x1, blocking collectives: none -> 33 us  [summed_on_arrival(): lax.all_to_all(blocks, axis, split_axis=0, concat_axis=0, tiled=True)]
    all_to_all x1, waiting for transfers between devices: 0.01 us -> 28 us  [from_everyone(): return lax.all_to_all(copies, axis, split_axis=0, concat_axis=0, tiled=True)]
    all_to_all x1, waiting for transfers between devices: 16.3 us -> 0.01 us  [shards(): lax.all_to_all(jnp.stack([mixer_piece] * lax.axis_size('tp')), 'tp', 0, 0)]
    all_to_all x1, starting transfers between devices: 16 us -> 3.47 us  [shards(): lax.all_to_all(jnp.stack([mixer_piece] * lax.axis_size('tp')), 'tp', 0, 0)]
where the time goes in v1:
time: 462 us; the launch traced here: 461 us
  blocking collectives  228 us (49%)
  waiting for transfers between devices  62.2 us (13%)
  local copies, waits for them, and re-layouts  55.8 us (12%)
  between operations  49.2 us (11%)
  other arithmetic  28.5 us (6%)
  starting transfers between devices  18.9 us (4%)
  matrix products  18.3 us (4%)
    all_to_all x1, blocking collectives, expert_half(): lax.all_to_all(outgoing, EP, split_axis=0, concat_axis=0, tiled=True)  107 us
    all_gather x2, blocking collectives, all_in_one(): both, at, found = (lax.all_gather(jnp.concatenate(lines), axis), 0, {})  88 us
    reduce_scatter x1, waiting for transfers between devices, shards(): lax.psum_scatter(expert_partial, 'tp', scatter_dimension=0, tiled=True)  34.1 us
    all_to_all x1, blocking collectives, summed_on_arrival(): lax.all_to_all(blocks, axis, split_axis=0, concat_axis=0, tiled=True)  33 us
    all_to_all x1, waiting for transfers between devices, from_everyone(): return lax.all_to_all(copies, axis, split_axis=0, concat_axis=0, tiled=True)  28 us
    gather x4, local copies, waits for them, and re-layouts, expert_half(): flat_back[gather_at[:, pick_index]].astype(jnp.float32)  23.9 us
    another operation x3, other arithmetic  18.2 us
  transfers between devices with their start and end apart: 4, of which 2 were waited for; matrix products, arithmetic and copies ran while one was open for 4% of the time, Pallas kernels for 0%

profile of v1, /device:TPU:1, one launch (start us, length us, event | category | flops | bytes accessed | tf_op | source)
XLA Modules:
  0.0 461.1 jit_solution(662745493397098917)
XLA Ops:
  7.2 0.9 copy.108
  8.6 18.0 %reduce-window.6 = s32[64,8,128]{2,1,0:T(8,128)S(1)} reduce-window(s32[64,8,128]{2,1,0:T(8,128)S(1)} %fusion.29, s32[]{:T(128)} %constant.140.clone.1), window={size=1x1x128 pad=0_0x0_0x127_0}, to_apply=%region_8.9 | reduce-window | flops 8323072 | bytes 524292 | tf_op jit(solution)/shard_map/reduce-window
  27.3 4.3 scatter_custom_fusion.1
  31.9 4.3 scatter_custom_fusion
  36.3 0.3 fusion.3
  36.6 6.0 %gather_fusion = bf16[1024,2048]{1,0:T(8,128)(2,1)} fusion(bf16[256,2048]{1,0:T(8,128)(2,1)S(1)} %fusion.3, s32[1024]{0:T(1024)S(1)} %fusion.157), kind=kCustom, calls=%fused_computation | custom fusion | bytes 8392704 | tf_op jit(solution)/shard_map/gather | solution.py:227
  42.7 2.5 broadcast_select_fusion
  45.2 107.2 %all_to_all.25 = bf16[32,32,2048]{2,1,0:T(8,128)(2,1)S(1)} all-to-all(bf16[32,32,2048]{2,1,0:T(8,128)(2,1)S(1)} %broadcast_select_fusion), channel_id=1, replica_groups=mesh['ep_0'=8,'ep_1'=4,'tp'=16] {'ep_0','ep_1'}, dimensions={0} | all-to-all | bytes 8388608 | tf_op jit(solution)/shard_map/all_to_all | solution.py:232
  152.5 1.9 copy-done.1
  154.4 1.2 fusion.18
  155.7 8.5 %convolution_convert_fusion = bf16[32,32,2048]{2,1,0:T(8,128)(2,1)} fusion(bf16[32,32,2048]{2,1,0:T(8,128)(2,1)} %copy-done.1, bf16[1,128,2048]{2,1,0:T(8,128)(2,1)S(1)} %copy-done, bf16[1,2048,128]{2,1,0:T(8,128)(2,1)S(1)} %copy-done.5, f32[32,32,128]{2,1,0:T(8,128)S(1)} %fusion.18), kind=kOutput, calls=%fused_computation.8 | convolution fusion | flops 1076625408 | bytes 9961472 | tf_op jit(solution)/shard_map/sif,fd->sid/dot_general | solution.py:236
  164.2 6.7 %all-to-all-start.3 = ((bf16[32,32,2048]{2,1,0:T(8,128)(2,1)}), bf16[32,32,2048]{2,1,0:T(8,128)(2,1)}, u32[]{:S(2)}, u32[]{:S(2)}) async-start(bf16[32,32,2048]{2,1,0:T(8,128)(2,1)} %convolution_convert_fusion), calls=%async_computation.3 | async-start | bytes 8388608 | tf_op jit(solution)/shard_map/all_to_all | solution.py:240
  171.2 0.3 reduce_window_sum.26
  171.5 0.6 slice.281
  172.7 1.2 fusion.178
  175.3 1.3 subtract_exponential_fusion.1
  177.1 0.6 pad_bitcast_fusion.3
  178.2 20.0 %all-gather.2 = f32[4,262,64]{1,2,0:T(8,128)S(1)} all-gather(f32[1,262,64]{1,2,0:T(8,128)S(1)} %maximum_bitcast_fusion), channel_id=2, replica_groups=mesh['ep_0'=8,'ep_1'=4,'tp'=16] {'ep_1'}, dimensions={0}, use_global_device_ids=true | all-gather | bytes 335360 | tf_op jit(solution)/shard_map/all_gather | solution.py:33
  198.5 0.6 fusion.185
  210.1 0.5 copy-done.7
  210.6 68.0 %all-gather.3 = f32[8,262,64]{1,2,0:T(8,128)S(1)} all-gather(f32[1,262,64]{1,2,0:T(8,128)S(1)} %maximum_bitcast_fusion.1), channel_id=3, replica_groups=mesh['ep_0'=8,'ep_1'=4,'tp'=16] {'ep_0'}, dimensions={0}, use_global_device_ids=true | all-gather | bytes 603648 | tf_op jit(solution)/shard_map/all_gather | solution.py:33
  278.8 0.7 copy.125
  279.5 1.6 fusion.184
  281.8 0.6 fusion.183
  303.2 0.7 broadcast_compare_fusion
  304.0 0.8 copy.120
  305.7 0.3 fusion.33
  306.0 0.6 pad_clamp_fusion.2
  306.6 0.6 pad_clamp_fusion
  307.3 0.9 slice_reduce_fusion.3
  308.2 1.0 fusion.188
  309.2 5.2 %gather_fusion.1 = bf16[256,2048]{1,0:T(8,128)(2,1)S(1)} fusion(bf16[1024,2048]{1,0:T(8,128)(2,1)} %bitcast.59, s32[1024]{0:T(1024)} %get-tuple-element.135), kind=kCustom, calls=%fused_computation.1 | custom fusion | bytes 2098176 | tf_op jit(solution)/shard_map/gather | solution.py:248
  314.4 6.2 %gather_fusion.2 = bf16[256,2048]{1,0:T(8,128)(2,1)} fusion(bf16[1024,2048]{1,0:T(8,128)(2,1)} %bitcast.59, s32[1024]{0:T(1024)} %get-tuple-element.134), kind=kCustom, calls=%fused_computation.2 | custom fusion | bytes 2098176 | tf_op jit(solution)/shard_map/gather | solution.py:248
  320.6 6.2 %gather_fusion.3 = bf16[256,2048]{1,0:T(8,128)(2,1)} fusion(bf16[1024,2048]{1,0:T(8,128)(2,1)} %bitcast.59, s32[1024]{0:T(1024)} %get-tuple-element.133), kind=kCustom, calls=%fused_computation.3 | custom fusion | bytes 2098176 | tf_op jit(solution)/shard_map/gather | solution.py:248
  326.9 6.2 %gather_fusion.4 = bf16[256,2048]{1,0:T(8,128)(2,1)} fusion(bf16[1024,2048]{1,0:T(8,128)(2,1)} %bitcast.59, s32[1024]{0:T(1024)} %get-tuple-element.132), kind=kCustom, calls=%fused_computation.4 | custom fusion | bytes 2098176 | tf_op jit(solution)/shard_map/gather | solution.py:248
  333.1 5.1 %convolution_add_fusion = f32[256,2048]{1,0:T(8,128)} fusion(bf16[32,2048]{1,0:T(8,128)(2,1)S(1)} %copy-done.9, bf16[256,2048]{1,0:T(8,128)(2,1)} %gather_fusion.4, bf16[256,2048]{1,0:T(8,128)(2,1)} %gather_fusion.3, bf16[256,2048]{1,0:T(8,128)(2,1)} %gather_fusion.2, bf16[256,2048]{1,0:T(8,128)(2,1)S(1)} %gather_fusion.1, bf16[256,2048]{1,0:T(8,128)(2,1)S(1)} %fusion.3, ...), kind=kOutput, calls=%fused_computation.9 | convolution fusion | flops 73449472 | bytes 7639040 | tf_op jit(solution)/shard_map/dot_general | solution.py:254
  340.3 1.3 convolution_multiply_fusion.4
  341.6 0.5 fusion
  342.1 33.0 %all_to_all.26 = bf16[16,8,2048]{2,1,0:T(8,128)(2,1)S(1)} all-to-all(bf16[16,8,2048]{2,1,0:T(8,128)(2,1)S(1)} %fusion), channel_id=1, replica_groups=mesh['ep_0'=8,'ep_1'=4,'tp'=16] {'tp'}, dimensions={0} | all-to-all | bytes 1048576 | tf_op jit(solution)/shard_map/all_to_all | solution.py:64
  375.2 0.8 stack.2
  376.1 3.5 all-to-all-start.1
  379.6 34.1 %reduce-scatter.2.cloned.1.call-done = f32[16,2048]{1,0:T(8,128)} async-done(((f32[256,2048]{1,0:T(8,128)}), f32[16,2048]{1,0:T(8,128)}) %reduce-scatter.2.cloned.1.call-update) | async-done | bytes 131088 | tf_op jit(solution)/shard_map/reduce_scatter | solution.py:297
  413.7 0.9 convert_element_type.83
  414.6 1.1 broadcast_in_dim.93
  415.7 8.8 %all-to-all-start.4 = ((bf16[16,16,2048]{2,1,0:T(8,128)(2,1)}), bf16[16,16,2048]{2,1,0:T(8,128)(2,1)S(1)}, u32[]{:S(2)}, u32[]{:S(2)}) async-start(bf16[16,16,2048]{2,1,0:T(8,128)(2,1)} %broadcast_in_dim.93), calls=%async_computation.5 | async-start | bytes 2097152 | tf_op jit(solution)/shard_map/all_to_all | solution.py:70
  424.5 28.0 %all-to-all-done.4 = bf16[16,16,2048]{2,1,0:T(8,128)(2,1)S(1)} async-done(((bf16[16,16,2048]{2,1,0:T(8,128)(2,1)}), bf16[16,16,2048]{2,1,0:T(8,128)(2,1)S(1)}, u32[]{:S(2)}, u32[]{:S(2)}) %all-to-all-start.4) | async-done | bytes 1048608 | tf_op jit(solution)/shard_map/all_to_all | solution.py:70
  452.5 0.8 copy.149
  453.2 1.0 copy.150
  (136 shorter events, 6.0 us)
Async XLA Ops:
  7.2 148.5 %copy-start = (bf16[1,128,2048]{2,1,0:T(8,128)(2,1)S(1)}, bf16[1,128,2048]{2,1,0:T(8,128)(2,1)}, u32[]{:S(2)}) copy-start(bf16[1,128,2048]{2,1,0:T(8,128)(2,1)} %param.30) | copy-start | bytes 1572868
  7.2 24.4 %copy-start.2 = (bf16[256,2048]{1,0:T(8,128)(2,1)S(1)}, bf16[256,2048]{1,0:T(8,128)(2,1)}, u32[]{:S(2)}) copy-start(bf16[256,2048]{1,0:T(8,128)(2,1)} %param.24) | copy-start | bytes 3145732
  7.2 29.1 %copy-start.26 = (f32[2048]{0:T(1024)S(1)}, f32[2048]{0:T(1024)}, u32[]{:S(2)}) copy-start(f32[2048]{0:T(1024)} %param.25) | copy-start | bytes 24580
  45.2 109.2 %copy-start.4 = (bf16[1,2048,128]{2,1,0:T(8,128)(2,1)S(1)}, bf16[1,2048,128]{2,1,0:T(8,128)(2,1)}, u32[]{:S(2)}) copy-start(bf16[1,2048,128]{2,1,0:T(8,128)(2,1)} %param.28) | copy-start | bytes 1572868
  152.5 1.9 copy-start.1
  154.4 1.3 copy-start.5
  164.2 6.9 %copy-start.29 = (f32[128,2]{0,1:T(2,128)S(1)}, f32[128,2]{0,1:T(2,128)}, u32[]{:S(2)}) copy-start(f32[128,2]{0,1:T(2,128)} %param.21) | copy-start | bytes 3076
  164.2 6.9 %copy-start.30 = (f32[128,2]{0,1:T(2,128)S(1)}, f32[128,2]{0,1:T(2,128)}, u32[]{:S(2)}) copy-start(f32[128,2]{0,1:T(2,128)} %param.22) | copy-start | bytes 3076
  164.2 12.5 %copy-start.11 = (bf16[128,512]{1,0:T(8,128)(2,1)S(1)}, bf16[128,512]{1,0:T(8,128)(2,1)}, u32[]{:S(2)}) copy-start(bf16[128,512]{1,0:T(8,128)(2,1)} %param.18) | copy-start | bytes 393220
  164.2 13.7 %copy-start.13 = (bf16[128,64]{0,1:T(8,128)(2,1)S(1)}, bf16[128,64]{0,1:T(8,128)(2,1)}, u32[]{:S(2)}) copy-start(bf16[128,64]{0,1:T(8,128)(2,1)} %param.19) | copy-start | bytes 49156
  164.2 145.0 %all-to-all-start.3 = ((bf16[32,32,2048]{2,1,0:T(8,128)(2,1)}), bf16[32,32,2048]{2,1,0:T(8,128)(2,1)}, u32[]{:S(2)}, u32[]{:S(2)}) async-start(bf16[32,32,2048]{2,1,0:T(8,128)(2,1)} %convolution_convert_fusion), calls=%async_computation.3 | async-start | bytes 8388608 | tf_op jit(solution)/shard_map/all_to_all | solution.py:240
  170.8 242.9 %reduce-scatter.2.cloned.1.call-start = ((), (), s32[]{:S(2)}) async-start(), calls=%async_computation.6 | async-start | bytes 2228224 | tf_op jit(solution)/shard_map/reduce_scatter | solution.py:297
  171.1 5.6 %copy-start.27 = (f32[128]{0:T(128)}, f32[128]{0:T(128)S(1)}, u32[]{:S(2)}) copy-start(f32[128]{0:T(128)S(1)} %get-tuple-element.69) | copy-start | bytes 1540
  171.5 6.3 %copy-start.24 = (f32[1,128]{1,0:T(1,128)}, f32[1,128]{1,0:T(1,128)S(1)}, u32[]{:S(2)}) copy-start(f32[1,128]{1,0:T(1,128)S(1)} %reduce_window_sum.26) | copy-start | bytes 1540
  198.2 102.5 %copy-start.3 = (f32[4,262,64]{1,2,0:T(8,128)}, f32[4,262,64]{1,2,0:T(8,128)S(1)}, u32[]{:S(2)}) copy-start(f32[4,262,64]{1,2,0:T(8,128)S(1)} %all-gather.2) | copy-start | bytes 804868
  208.1 1.7 copy-start.15
  208.2 1.6 copy-start.17
  208.3 1.5 copy-start.19
  208.4 1.5 copy-start.21
  210.0 0.6 copy-start.7
  279.5 28.6 %copy-start.10 = (bf16[2048,32]{0,1:T(8,128)(2,1)S(1)}, bf16[2048,32]{0,1:T(8,128)(2,1)}, u32[]{:S(2)}) copy-start(bf16[2048,32]{0,1:T(8,128)(2,1)} %param.31) | copy-start | bytes 393220
  326.9 6.2 %copy-start.9 = (bf16[32,2048]{1,0:T(8,128)(2,1)S(1)}, bf16[32,2048]{1,0:T(8,128)(2,1)}, u32[]{:S(2)}) copy-start(bf16[32,2048]{1,0:T(8,128)(2,1)} %param.33) | copy-start | bytes 393220
  338.2 1.2 copy-start.16
  338.2 1.2 copy-start.18
  338.2 1.3 copy-start.20
  338.2 1.3 copy-start.22
  338.2 1.5 copy-start.25
  338.2 1.5 copy-start.28
  338.2 1.7 copy-start.12
  338.2 1.7 copy-start.14
  338.3 2.0 copy-start.8
  338.3 3.4 copy-start.6
  338.3 3.4 copy-start.23
  376.1 38.5 %all-to-all-start.1 = ((bf16[16,8,2048]{2,1,0:T(8,128)(2,1)}), bf16[16,8,2048]{2,1,0:T(8,128)(2,1)S(1)}, u32[]{:S(2)}, u32[]{:S(2)}) async-start(bf16[16,8,2048]{2,1,0:T(8,128)(2,1)} %stack.2), calls=%async_computation.1 | async-start | bytes 1048576 | tf_op jit(solution)/shard_map/all_to_all | solution.py:295
  415.7 36.7 %all-to-all-start.4 = ((bf16[16,16,2048]{2,1,0:T(8,128)(2,1)}), bf16[16,16,2048]{2,1,0:T(8,128)(2,1)S(1)}, u32[]{:S(2)}, u32[]{:S(2)}) async-start(bf16[16,16,2048]{2,1,0:T(8,128)(2,1)} %broadcast_in_dim.93), calls=%async_computation.5 | async-start | bytes 2097152 | tf_op jit(solution)/shard_map/all_to_all | solution.py:70
Sparse Core Ops, SparseCore 0:
  338.4 75.2 reduce-scatter.1
